TPU v7x, 128 devices: a whole 4x4x4 slice. The times are simulated.
128 devices in a mesh: fs: 16 (over z, y), tp: 8 (over x, core).
Axes of the slice: x: 4, y: 4, z: 4, core: 2. Of those that a mesh axis runs over, the one named last changes fastest.
Arguments:
- saved_input: bfloat16 [262144, 2048], P(('fs', 'tp')), may hold values from -500 to 500
- value_cotangent: bfloat16 [262144, 1024], P(('fs', 'tp')), may hold values from -500 to 500
- hidden_input: bfloat16 [262144, 1024], P(('fs', 'tp')), may hold values from -500 to 500
- out_cotangent: bfloat16 [262144, 2048], P(('fs', 'tp')), may hold values from -500 to 500
- value_factor: bfloat16 [2048, 256], P('fs'), may hold values from -2 to 2
- out_factor: bfloat16 [1024, 256], P('fs'), may hold values from -2 to 2
- value_weight: float32 [2048, 1024], P('fs', 'tp'), may hold values from -0.125 to 0.125
- out_weight: float32 [1024, 2048], P('fs', 'tp'), may hold values from -0.1875 to 0.1875
- value_first: float32 [256, 1024], P('fs', 'tp'), may hold values from -1.2 to 1.2
- value_second: float32 [256, 1024], P('fs', 'tp'), may hold values from 0.02 to 0.5
- out_first: float32 [256, 2048], P('fs', 'tp'), may hold values from -1.2 to 1.2
- out_second: float32 [256, 2048], P('fs', 'tp'), may hold values from 0.02 to 0.5
Outputs:
- value_update: float32 [2048, 1024], P('fs', 'tp')
- out_update: float32 [1024, 2048], P('fs', 'tp')
- new_value_weight: float32 [2048, 1024], P('fs', 'tp')
- new_out_weight: float32 [1024, 2048], P('fs', 'tp')
- value_copy: bfloat16 [2048, 1024], P(None, 'tp')
- out_copy: bfloat16 [1024, 2048], P(None, 'tp')
- new_value_first: float32 [256, 1024], P('fs', 'tp')
- new_value_second: float32 [256, 1024], P('fs', 'tp')
- new_out_first: float32 [256, 2048], P('fs', 'tp')
- new_out_second: float32 [256, 2048], P('fs', 'tp')
All inputs are finite; a program needn't handle non-finite values.
Results may differ from a plain program's by a relative error of at most 0.0065.
Values may be sent and summed in bfloat16 or wider, within the bound.
No kernel may reach another device: no remote copies, remote signals or barrier semaphores. Data moves between devices by JAX's collectives and lax.ppermute only.
A program may use at most 128 MiB of HBM per device.

v0:
```python
import jax
import jax.numpy as jnp
from jax import lax
from jax.sharding import Mesh
from jax.sharding import PartitionSpec as P

D = 2048
DM = 1024
R = 256
FS = ("fs_0", "fs_1")
TP = ("tp_0", "tp_1")
FS_TP = ("fs_0", "fs_1", "tp_0", "tp_1")
momentum_decay = 0.9
square_decay = 0.95
adam_epsilon = 1e-08
update_scale = 0.25
learning_rate = 0.01


def copy_for_each(shard, axis):
    copies = jnp.broadcast_to(shard, (lax.axis_size(axis), *shard.shape))
    return lax.all_to_all(copies, axis, split_axis=0, concat_axis=0, tiled=True)


def laid_out(tiles, dim):
    tiles = jnp.moveaxis(tiles, 0, dim)
    lengths = tiles.shape
    return tiles.reshape(*lengths[:dim], lengths[dim] * lengths[dim + 1], *lengths[dim + 2 :])


def collect(shard, axis, dim):
    tiles = copy_for_each(shard, axis)
    return laid_out(tiles, dim)


def split_up(shard, dim, length):
    before, after = (shard.shape[:dim], shard.shape[dim + 1 :])
    return jnp.moveaxis(shard.reshape(*before, length, -1, *after), dim, 0)


def sum_at_owner(shard, axis, dim):
    length = lax.axis_size(axis)
    tiles = lax.all_to_all(split_up(shard, dim, length), axis, 0, 0, tiled=True)
    return jnp.sum(tiles.astype(jnp.float32), axis=0)


def sum_at_owner_2(shard, axis, dim):
    tiles = split_up(shard, dim, lax.axis_size(axis))
    arrived = lax.all_to_all(tiles, axis, split_axis=0, concat_axis=0, tiled=True)
    return arrived.sum(axis=0)


def over_axes(shard, axes):
    for axis in axes:
        shard = lax.psum(shard, axis)
    return shard


def side_by_side(arrays, axis, dim, along):
    ends, at = ([], 0)
    for a in arrays[:-1]:
        at += a.shape[along]
        ends.append(at)
    both = jnp.concatenate(arrays, axis=along)
    return tuple(jnp.split(lax.all_gather(both, axis, axis=dim, tiled=True), ends, axis=along))


def gather_packed(arrays, axis, dims):
    flat = jnp.concatenate([a.reshape(-1) for a in arrays])
    lines, at, outs = (lax.all_gather(flat, axis), 0, [])
    for a, dim in zip(arrays, dims):
        tiles = lines[:, at : at + a.size].reshape(-1, *a.shape)
        outs.append(laid_out(tiles, dim))
        at += a.size
    return tuple(outs)


def moment_ratio(first, second, lowrank, clip_factor):
    scaled = clip_factor * lowrank
    new_first = momentum_decay * first + (1.0 - momentum_decay) * scaled
    new_second = square_decay * second + (1.0 - square_decay) * scaled * scaled
    ratio = new_first / (jnp.sqrt(new_second) + adam_epsilon)
    return (new_first, new_second, ratio)


def input_times_factor(inputs, factor):
    return jnp.dot(inputs, collect(factor, FS, 0), preferred_element_type=jnp.float32)


def split_product(basis, cotangents):
    basis_high = basis.astype(jnp.bfloat16)
    basis_rest = (basis - basis_high.astype(jnp.float32)).astype(jnp.bfloat16)
    high_part = jnp.einsum("tr,tc->rc", basis_high, cotangents, preferred_element_type=jnp.float32)
    rest_part = jnp.einsum("tr,tc->rc", basis_rest, cotangents, preferred_element_type=jnp.float32)
    return high_part + rest_part


def shards(
    saved_input,
    value_cotangent,
    hidden_input,
    out_cotangent,
    value_factor,
    out_factor,
    value_weight,
    out_weight,
    value_first,
    value_second,
    out_first,
    out_second,
):
    highest = lax.Precision.HIGHEST
    value_basis = input_times_factor(saved_input, value_factor)
    out_basis = input_times_factor(hidden_input, out_factor)
    left = value_basis
    right = out_basis
    first_part = split_product(left, value_cotangent)
    second_part = split_product(right, out_cotangent)
    lowrank = sum_at_owner(
        jnp.concatenate([first_part, second_part], axis=1).astype(jnp.bfloat16), FS, 0
    )
    low_value, low_out = (
        sum_at_owner_2(lowrank[:, :DM], TP, 1),
        sum_at_owner_2(lowrank[:, DM:], TP, 1),
    )
    squares = (
        over_axes(jnp.sum(low_value * low_value), FS_TP),
        over_axes(jnp.sum(low_out * low_out), FS_TP),
    )
    root_mean = jnp.sqrt((squares[0] + squares[1]) / (R * (D + DM)))
    clip_factor = 1.0 / jnp.maximum(root_mean, 1.0)
    new_value_first, new_value_second, value_ratio = moment_ratio(
        value_first, value_second, low_value, clip_factor
    )
    new_out_first, new_out_second, out_ratio = moment_ratio(
        out_first, out_second, low_out, clip_factor
    )
    pieces = side_by_side((value_ratio, out_ratio), FS, 0, 1)
    left = value_factor.astype(jnp.float32)
    right = out_factor.astype(jnp.float32)
    value_sum = jnp.dot(left, pieces[0], precision=highest)
    out_sum = jnp.dot(right, pieces[1], precision=highest)
    value_update = update_scale * value_sum
    out_update = update_scale * out_sum
    new_value_weight = value_weight - learning_rate * value_update
    new_out_weight = out_weight - learning_rate * out_update
    value_copy, out_copy = gather_packed(
        (new_value_weight.astype(jnp.bfloat16), new_out_weight.astype(jnp.bfloat16)), FS, (0, 0)
    )
    return (
        value_update,
        out_update,
        new_value_weight,
        new_out_weight,
        value_copy,
        out_copy,
        new_value_first,
        new_value_second,
        new_out_first,
        new_out_second,
    )


def solution(mesh):
    torus = Mesh(mesh.devices.reshape(4, 4, 4, 2), ("fs_0", "fs_1", "tp_0", "tp_1"))
    return jax.shard_map(
        shards,
        mesh=torus,
        in_specs=(
            P(FS_TP, None),
            P(FS_TP, None),
            P(FS_TP, None),
            P(FS_TP, None),
            P(FS, None),
            P(FS, None),
            P(FS, TP),
            P(FS, TP),
            P(FS, TP),
            P(FS, TP),
            P(FS, TP),
            P(FS, TP),
        ),
        out_specs=(
            P(FS, TP),
            P(FS, TP),
            P(FS, TP),
            P(FS, TP),
            P(None, TP),
            P(None, TP),
            P(FS, TP),
            P(FS, TP),
            P(FS, TP),
            P(FS, TP),
        ),
        check_vma=False,
    )
```

profile of v0, /device:TPU:0, one launch (start us, length us, event | category | flops | bytes accessed | tf_op | source)
XLA Modules:
  0.0 212.2 jit_solution(17302194149277601238)
XLA Ops:
  8.0 19.5 %all_to_all.25 = bf16[16,64,256]{2,1,0:T(8,128)(2,1)S(1)} all-to-all(bf16[16,64,256]{2,1,0:T(8,128)(2,1)S(1)} %broadcast_in_dim.7), channel_id=1, replica_groups=mesh['fs_0'=4,'fs_1'=4,'tp_0'=4,'tp_1'=2] {'fs_0','fs_1'}, dimensions={0} | all-to-all | bytes 1048576 | tf_op jit(solution)/shard_map/all_to_all | solution.py:22
  27.5 1.9 broadcast_in_dim.6
  29.4 3.7 %all-to-all-start = ((bf16[16,128,256]{2,1,0:T(8,128)(2,1)}), bf16[16,128,256]{2,1,0:T(8,128)(2,1)S(1)}, u32[]{:S(2)}, u32[]{:S(2)}) async-start(bf16[16,128,256]{2,1,0:T(8,128)(2,1)} %broadcast_in_dim.6), calls=%async_computation | async-start | bytes 2097152 | tf_op jit(solution)/shard_map/all_to_all | solution.py:22
  33.1 3.6 %fusion.19 = f32[2048,256]{1,0:T(8,128)S(1)} fusion(bf16[2048,1024]{1,0:T(8,128)(2,1)} %param.14, bf16[1024,256]{1,0:T(8,128)(2,1)S(1)} %bitcast.41), kind=kOutput, calls=%fused_computation.39 | convolution fusion | flops 1073741824 | bytes 6815744 | tf_op jit(solution)/shard_map/dot_general | solution.py:87
  36.7 5.9 %fusion.3 = f32[256,2048]{1,0:T(8,128)S(1)} fusion(bf16[2048,2048]{1,0:T(8,128)(2,1)} %param.15, f32[2048,256]{1,0:T(8,128)S(1)} %fusion.19), kind=kOutput, calls=%fused_computation.9 | convolution fusion | flops 2148007936 | bytes 12582912 | tf_op jit(solution)/shard_map/tr,tc->rc/dot_general | solution.py:93
  42.6 2.4 %fusion = bf16[256,2048]{1,0:T(8,128)(2,1)S(1)} fusion(f32[256,2048]{1,0:T(8,128)S(1)} %fusion.3, bf16[2048,2048]{1,0:T(8,128)(2,1)S(1)} %bitcast.38, f32[2048,256]{1,0:T(8,128)S(1)} %fusion.19), kind=kOutput, calls=%fused_computation.2 | convolution fusion | flops 2150629376 | bytes 13631488 | tf_op jit(solution)/shard_map/tr,tc->rc/dot_general | solution.py:94
  45.0 4.4 %all-to-all-done = bf16[16,128,256]{2,1,0:T(8,128)(2,1)S(1)} async-done(((bf16[16,128,256]{2,1,0:T(8,128)(2,1)}), bf16[16,128,256]{2,1,0:T(8,128)(2,1)S(1)}, u32[]{:S(2)}, u32[]{:S(2)}) %all-to-all-start) | async-done | bytes 1048608 | tf_op jit(solution)/shard_map/all_to_all | solution.py:22
  49.4 6.0 %fusion.18 = f32[2048,256]{1,0:T(8,128)S(1)} fusion(bf16[2048,2048]{1,0:T(8,128)(2,1)} %param.12, bf16[2048,256]{1,0:T(8,128)(2,1)S(1)} %bitcast.40), kind=kOutput, calls=%fused_computation.38 | convolution fusion | flops 2147483648 | bytes 11534336 | tf_op jit(solution)/shard_map/dot_general | solution.py:87
  55.4 1.3 fusion.6
  56.7 1.3 fusion.1
  58.1 25.1 %all_to_all.26 = bf16[16,16,3072]{2,1,0:T(8,128)(2,1)S(1)} all-to-all(bf16[16,16,3072]{2,1,0:T(8,128)(2,1)S(1)} %pad_maximum_fusion), channel_id=1, replica_groups=mesh['fs_0'=4,'fs_1'=4,'tp_0'=4,'tp_1'=2] {'fs_0','fs_1'}, dimensions={0} | all-to-all | bytes 3145728 | tf_op jit(solution)/shard_map/all_to_all | solution.py:43
  84.2 4.3 %all-to-all-start.3 = ((f32[8,16,128]{2,1,0:T(8,128)}), f32[8,16,128]{2,1,0:T(8,128)S(1)}, u32[]{:S(2)}, u32[]{:S(2)}) async-start(f32[8,16,128]{2,1,0:T(8,128)} %copy.33), calls=%async_computation.3 | async-start | bytes 131072 | tf_op jit(solution)/shard_map/all_to_all | solution.py:49
  89.2 4.9 %all-to-all-done.3 = f32[8,16,128]{2,1,0:T(8,128)S(1)} async-done(((f32[8,16,128]{2,1,0:T(8,128)}), f32[8,16,128]{2,1,0:T(8,128)S(1)}, u32[]{:S(2)}, u32[]{:S(2)}) %all-to-all-start.3) | async-done | bytes 65568 | tf_op jit(solution)/shard_map/all_to_all | solution.py:49
  94.1 3.4 %all-to-all-start.4 = ((f32[8,16,256]{2,1,0:T(8,128)}), f32[8,16,256]{2,1,0:T(8,128)S(1)}, u32[]{:S(2)}, u32[]{:S(2)}) async-start(f32[8,16,256]{2,1,0:T(8,128)} %copy.34), calls=%async_computation.4 | async-start | bytes 262144 | tf_op jit(solution)/shard_map/all_to_all | solution.py:49
  98.1 5.4 %all-to-all-done.4 = f32[8,16,256]{2,1,0:T(8,128)S(1)} async-done(((f32[8,16,256]{2,1,0:T(8,128)}), f32[8,16,256]{2,1,0:T(8,128)S(1)}, u32[]{:S(2)}, u32[]{:S(2)}) %all-to-all-start.4) | async-done | bytes 131104 | tf_op jit(solution)/shard_map/all_to_all | solution.py:49
  105.4 9.1 %psum.67 = f32[]{:T(128)} all-reduce(f32[]{:T(128)S(6)} %add.51), channel_id=1, replica_groups=mesh['fs_0'=4,'fs_1'=4,'tp_0'=4,'tp_1'=2] {'fs_0'}, use_global_device_ids=true, to_apply=%region_3.0 | all-reduce | flops 1 | bytes 8 | tf_op jit(solution)/shard_map/psum | solution.py:55
  114.5 9.2 %psum.66 = f32[]{:T(128)} all-reduce(f32[]{:T(128)} %psum.67), channel_id=1, replica_groups=mesh['fs_0'=4,'fs_1'=4,'tp_0'=4,'tp_1'=2] {'fs_1'}, use_global_device_ids=true, to_apply=%region_4.0 | all-reduce | flops 1 | bytes 8 | tf_op jit(solution)/shard_map/psum | solution.py:55
  123.7 9.5 %psum.65 = f32[]{:T(128)} all-reduce(f32[]{:T(128)} %psum.66), channel_id=1, replica_groups=mesh['fs_0'=4,'fs_1'=4,'tp_0'=4,'tp_1'=2] {'tp_0'}, use_global_device_ids=true, to_apply=%region_5.0 | all-reduce | flops 1 | bytes 8 | tf_op jit(solution)/shard_map/psum | solution.py:55
  133.3 3.1 %psum.64 = f32[]{:T(128)} all-reduce(f32[]{:T(128)} %psum.65), channel_id=1, replica_groups=mesh['fs_0'=4,'fs_1'=4,'tp_0'=4,'tp_1'=2] {'tp_1'}, use_global_device_ids=true, to_apply=%region_6.0 | all-reduce | flops 1 | bytes 8 | tf_op jit(solution)/shard_map/psum | solution.py:55
  138.4 22.0 %all_gather.9 = f32[256,384]{1,0:T(8,128)S(1)} all-gather(f32[16,384]{1,0:T(8,128)S(1)} %pad_maximum_fusion.2), channel_id=1, replica_groups=mesh['fs_0'=4,'fs_1'=4,'tp_0'=4,'tp_1'=2] {'fs_0','fs_1'}, dimensions={0}, use_global_device_ids=true | all-gather | bytes 417792 | tf_op jit(solution)/shard_map/all_gather | solution.py:65
  164.5 37.2 %all-gather.3.cloned.1.call-done = bf16[524288]{0:T(1024)(128)(2,1)} async-done(((bf16[32768]{0:T(1024)(128)(2,1)}), bf16[524288]{0:T(1024)(128)(2,1)}) %all-gather.3.cloned.1.call-update) | async-done | bytes 1048592 | tf_op jit(solution)/shard_map/all_gather | solution.py:70
  201.7 1.5 reshape.49
  203.3 1.0 reshape_reshape.6
  204.4 1.0 reshape_reshape.7
  (53 shorter events, 9.3 us)
Async XLA Ops:
  29.4 19.9 %all-to-all-start = ((bf16[16,128,256]{2,1,0:T(8,128)(2,1)}), bf16[16,128,256]{2,1,0:T(8,128)(2,1)S(1)}, u32[]{:S(2)}, u32[]{:S(2)}) async-start(bf16[16,128,256]{2,1,0:T(8,128)(2,1)} %broadcast_in_dim.6), calls=%async_computation | async-start | bytes 2097152 | tf_op jit(solution)/shard_map/all_to_all | solution.py:22
  33.1 9.5 %slice-start = ((s8[8388608]{0:T(1024)(128)(4,1)}), s8[4194304]{0:T(1024)(128)(4,1)S(1)}, s32[]{:S(2)}) async-start(s8[8388608]{0:T(1024)(128)(4,1)} %bitcast.37), calls=%async_computation.6 | async-start | bytes 8388608
  36.7 5.9 %slice-start.1 = ((s8[8388608]{0:T(1024)(128)(4,1)}), s8[4194304]{0:T(1024)(128)(4,1)S(1)}, s32[]{:S(2)}) async-start(s8[8388608]{0:T(1024)(128)(4,1)} %bitcast.37), calls=%async_computation.7 | async-start | bytes 8388608
  49.4 6.0 %copy-start.8 = (bf16[2048,1024]{1,0:T(8,128)(2,1)S(1)}, bf16[2048,1024]{1,0:T(8,128)(2,1)}, u32[]{:S(2)}) copy-start(bf16[2048,1024]{1,0:T(8,128)(2,1)} %param.13) | copy-start | bytes 12582916
  83.2 50.0 %copy-start.3 = (f32[128,128]{1,0:T(8,128)S(1)}, f32[128,128]{1,0:T(8,128)}, u32[]{:S(2)}) copy-start(f32[128,128]{1,0:T(8,128)} %param.18) | copy-start | bytes 196612
  83.2 53.9 %copy-start.4 = (f32[16,256]{1,0:T(8,128)S(1)}, f32[16,256]{1,0:T(8,128)}, u32[]{:S(2)}) copy-start(f32[16,256]{1,0:T(8,128)} %param.23) | copy-start | bytes 49156
  83.2 54.0 %copy-start.5 = (f32[16,256]{1,0:T(8,128)S(1)}, f32[16,256]{1,0:T(8,128)}, u32[]{:S(2)}) copy-start(f32[16,256]{1,0:T(8,128)} %param.22) | copy-start | bytes 49156
  83.2 54.6 %copy-start.6 = (f32[16,128]{1,0:T(8,128)S(1)}, f32[16,128]{1,0:T(8,128)}, u32[]{:S(2)}) copy-start(f32[16,128]{1,0:T(8,128)} %param.21) | copy-start | bytes 24580
  83.2 54.6 %copy-start.7 = (f32[16,128]{1,0:T(8,128)S(1)}, f32[16,128]{1,0:T(8,128)}, u32[]{:S(2)}) copy-start(f32[16,128]{1,0:T(8,128)} %param.20) | copy-start | bytes 24580
  83.2 77.1 %copy-start.1 = (bf16[64,256]{1,0:T(8,128)(2,1)S(1)}, bf16[64,256]{1,0:T(8,128)(2,1)}, u32[]{:S(2)}) copy-start(bf16[64,256]{1,0:T(8,128)(2,1)} %param.17) | copy-start | bytes 98308
  83.2 77.4 %copy-start = (bf16[128,256]{1,0:T(8,128)(2,1)S(1)}, bf16[128,256]{1,0:T(8,128)(2,1)}, u32[]{:S(2)}) copy-start(bf16[128,256]{1,0:T(8,128)(2,1)} %param.16) | copy-start | bytes 196612
  83.5 77.4 %copy-start.2 = (f32[64,256]{1,0:T(8,128)S(1)}, f32[64,256]{1,0:T(8,128)}, u32[]{:S(2)}) copy-start(f32[64,256]{1,0:T(8,128)} %param.19) | copy-start | bytes 196612
  84.2 9.9 %all-to-all-start.3 = ((f32[8,16,128]{2,1,0:T(8,128)}), f32[8,16,128]{2,1,0:T(8,128)S(1)}, u32[]{:S(2)}, u32[]{:S(2)}) async-start(f32[8,16,128]{2,1,0:T(8,128)} %copy.33), calls=%async_computation.3 | async-start | bytes 131072 | tf_op jit(solution)/shard_map/all_to_all | solution.py:49
  94.1 9.4 %all-to-all-start.4 = ((f32[8,16,256]{2,1,0:T(8,128)}), f32[8,16,256]{2,1,0:T(8,128)S(1)}, u32[]{:S(2)}, u32[]{:S(2)}) async-start(f32[8,16,256]{2,1,0:T(8,128)} %copy.34), calls=%async_computation.4 | async-start | bytes 262144 | tf_op jit(solution)/shard_map/all_to_all | solution.py:49
  97.5 104.3 %all-gather.3.cloned.1.call-start = ((), (), s32[]{:S(2)}) async-start(), calls=%async_computation.5 | async-start | bytes 1114112 | tf_op jit(solution)/shard_map/all_gather | solution.py:70
Sparse Core Ops, SparseCore 0:
  162.5 39.1 all-gather.2
where the time goes:
time: 213 us; the launch traced here: 212 us
  blocking collectives  97.5 us (46%)
  waiting for transfers between devices  51.9 us (24%)
  matrix products  20.9 us (10%)
  between operations  16.4 us (8%)
  starting transfers between devices  11.4 us (5%)
  local copies, waits for them, and re-layouts  9.54 us (4%)
  other arithmetic  4.73 us (2%)
    all_gather x1, waiting for transfers between devices, gather_packed(): lines, at, outs = (lax.all_gather(flat, axis), 0, [])  37.2 us
    psum x4, blocking collectives, over_axes(): shard = lax.psum(shard, axis)  30.9 us
    all_to_all x1, blocking collectives, sum_at_owner(): tiles = lax.all_to_all(split_up(shard, dim, length), axis, 0, 0, tiled=True)  25.1 us
    all_gather x1, blocking collectives, side_by_side(): lax.all_gather(both, axis, axis=dim, tiled=True)  22 us
    all_to_all x1, blocking collectives, copy_for_each(): return lax.all_to_all(copies, axis, split_axis=0, concat_axis=0, tiled=True)  19.5 us
    all_to_all x2, waiting for transfers between devices, sum_at_owner_2(): lax.all_to_all(tiles, axis, split_axis=0, concat_axis=0, tiled=True)  10.2 us
    dot_general x2, matrix products, input_times_factor(): jnp.dot(inputs, collect(factor, FS, 0), preferred_element_type=jnp.float32)  9.6 us
    all_to_all x2, starting transfers between devices, sum_at_owner_2(): lax.all_to_all(tiles, axis, split_axis=0, concat_axis=0, tiled=True)  7.67 us
  transfers between devices with their start and end apart: 4, of which 4 were waited for; matrix products, arithmetic and copies ran while one was open for 7% of the time, Pallas kernels for 0%

commit v1 on v0

--- a/solution.py
+++ b/solution.py
@@ -52,7 +52,7 @@
 
 def over_axes(shard, axes):
     for axis in axes:
-        shard = lax.psum(shard, axis)
+        shard = jnp.sum(lax.all_gather(shard, axis), axis=0)
     return shard
 
 

time: 213 us -> 227 us (1.066)
  local copies, waits for them, and re-layouts: 9.54 us -> 23.1 us
  other arithmetic: 4.73 us -> 9.54 us
  blocking collectives: 97.5 us -> 95.2 us
    psum x4 -> x0, blocking collectives: 30.9 us -> none  [over_axes(): shard = lax.psum(shard, axis)]
    unnamed x0 -> x4, blocking collectives: none -> 28.6 us
    unnamed x29 -> x57, local copies, waits for them, and re-layouts: 1.7 us -> 15.3 us
    reduce_sum x0 -> x8, other arithmetic: none -> 4.81 us  [over_axes(): shard = jnp.sum(lax.all_gather(shard, axis), axis=0)]
  transfers between devices with their start and end apart: 4 -> 4, of which waited for: 4 -> 4; matrix products, arithmetic and copies ran while one was open for 7% -> 8% of each run, Pallas kernels for 0% -> 0%
where the time goes in v1:
time: 227 us; the launch traced here: 226 us
  blocking collectives  95.2 us (42%)
  waiting for transfers between devices  49.9 us (22%)
  local copies, waits for them, and re-layouts  23.1 us (10%)
  matrix products  20.9 us (9%)
  between operations  15.8 us (7%)
  starting transfers between devices  11.4 us (5%)
  other arithmetic  9.54 us (4%)
    all_gather x1, waiting for transfers between devices, gather_packed(): lines, at, outs = (lax.all_gather(flat, axis), 0, [])  37.2 us
    unnamed x4, blocking collectives  28.6 us
    all_to_all x1, blocking collectives, sum_at_owner(): tiles = lax.all_to_all(split_up(shard, dim, length), axis, 0, 0, tiled=True)  25.2 us
    all_gather x1, blocking collectives, side_by_side(): lax.all_gather(both, axis, axis=dim, tiled=True)  22 us
    all_to_all x1, blocking collectives, copy_for_each(): return lax.all_to_all(copies, axis, split_axis=0, concat_axis=0, tiled=True)  19.5 us
    unnamed x57, local copies, waits for them, and re-layouts  15.3 us
    dot_general x2, matrix products, input_times_factor(): jnp.dot(inputs, collect(factor, FS, 0), preferred_element_type=jnp.float32)  9.59 us
    all_to_all x2, waiting for transfers between devices, sum_at_owner_2(): lax.all_to_all(tiles, axis, split_axis=0, concat_axis=0, tiled=True)  8.22 us
  transfers between devices with their start and end apart: 4, of which 4 were waited for; matrix products, arithmetic and copies ran while one was open for 8% of the time, Pallas kernels for 0%

profile of v1, /device:TPU:0, one launch (start us, length us, event | category | flops | bytes accessed | tf_op | source)
XLA Modules:
  0.0 225.8 jit_solution(3328762545576842187)
XLA Ops:
  8.0 19.5 %all_to_all.25 = bf16[16,64,256]{2,1,0:T(8,128)(2,1)S(1)} all-to-all(bf16[16,64,256]{2,1,0:T(8,128)(2,1)S(1)} %broadcast_in_dim.7), channel_id=1, replica_groups=mesh['fs_0'=4,'fs_1'=4,'tp_0'=4,'tp_1'=2] {'fs_0','fs_1'}, dimensions={0} | all-to-all | bytes 1048576 | tf_op jit(solution)/shard_map/all_to_all | solution.py:22
  27.5 1.9 broadcast_in_dim.6
  29.4 3.7 %all-to-all-start = ((bf16[16,128,256]{2,1,0:T(8,128)(2,1)}), bf16[16,128,256]{2,1,0:T(8,128)(2,1)S(1)}, u32[]{:S(2)}, u32[]{:S(2)}) async-start(bf16[16,128,256]{2,1,0:T(8,128)(2,1)} %broadcast_in_dim.6), calls=%async_computation | async-start | bytes 2097152 | tf_op jit(solution)/shard_map/all_to_all | solution.py:22
  33.1 3.6 %fusion.19 = f32[2048,256]{1,0:T(8,128)S(1)} fusion(bf16[2048,1024]{1,0:T(8,128)(2,1)} %param.14, bf16[1024,256]{1,0:T(8,128)(2,1)S(1)} %bitcast.53), kind=kOutput, calls=%fused_computation.39 | convolution fusion | flops 1073741824 | bytes 6815744 | tf_op jit(solution)/shard_map/dot_general | solution.py:87
  36.7 5.9 %fusion.3 = f32[256,2048]{1,0:T(8,128)S(1)} fusion(bf16[2048,2048]{1,0:T(8,128)(2,1)} %param.15, f32[2048,256]{1,0:T(8,128)S(1)} %fusion.19), kind=kOutput, calls=%fused_computation.9 | convolution fusion | flops 2148007936 | bytes 12582912 | tf_op jit(solution)/shard_map/tr,tc->rc/dot_general | solution.py:93
  42.6 2.4 %fusion = bf16[256,2048]{1,0:T(8,128)(2,1)S(1)} fusion(f32[256,2048]{1,0:T(8,128)S(1)} %fusion.3, bf16[2048,2048]{1,0:T(8,128)(2,1)S(1)} %bitcast.50, f32[2048,256]{1,0:T(8,128)S(1)} %fusion.19), kind=kOutput, calls=%fused_computation.2 | convolution fusion | flops 2150629376 | bytes 13631488 | tf_op jit(solution)/shard_map/tr,tc->rc/dot_general | solution.py:94
  45.0 4.4 %all-to-all-done = bf16[16,128,256]{2,1,0:T(8,128)(2,1)S(1)} async-done(((bf16[16,128,256]{2,1,0:T(8,128)(2,1)}), bf16[16,128,256]{2,1,0:T(8,128)(2,1)S(1)}, u32[]{:S(2)}, u32[]{:S(2)}) %all-to-all-start) | async-done | bytes 1048608 | tf_op jit(solution)/shard_map/all_to_all | solution.py:22
  49.4 6.0 %fusion.18 = f32[2048,256]{1,0:T(8,128)S(1)} fusion(bf16[2048,2048]{1,0:T(8,128)(2,1)} %param.12, bf16[2048,256]{1,0:T(8,128)(2,1)S(1)} %bitcast.52), kind=kOutput, calls=%fused_computation.38 | convolution fusion | flops 2147483648 | bytes 11534336 | tf_op jit(solution)/shard_map/dot_general | solution.py:87
  58.1 25.2 %all_to_all.26 = bf16[16,16,3072]{2,1,0:T(8,128)(2,1)S(1)} all-to-all(bf16[16,16,3072]{2,1,0:T(8,128)(2,1)S(1)} %pad_maximum_fusion), channel_id=1, replica_groups=mesh['fs_0'=4,'fs_1'=4,'tp_0'=4,'tp_1'=2] {'fs_0','fs_1'}, dimensions={0} | all-to-all | bytes 3145728 | tf_op jit(solution)/shard_map/all_to_all | solution.py:43
  84.2 4.3 %all-to-all-start.3 = ((f32[8,16,128]{2,1,0:T(8,128)}), f32[8,16,128]{2,1,0:T(8,128)S(1)}, u32[]{:S(2)}, u32[]{:S(2)}) async-start(f32[8,16,128]{2,1,0:T(8,128)} %copy.33), calls=%async_computation.3 | async-start | bytes 131072 | tf_op jit(solution)/shard_map/all_to_all | solution.py:49
  89.3 4.9 %all-to-all-done.3 = f32[8,16,128]{2,1,0:T(8,128)S(1)} async-done(((f32[8,16,128]{2,1,0:T(8,128)}), f32[8,16,128]{2,1,0:T(8,128)S(1)}, u32[]{:S(2)}, u32[]{:S(2)}) %all-to-all-start.3) | async-done | bytes 65568 | tf_op jit(solution)/shard_map/all_to_all | solution.py:49
  94.1 3.4 %all-to-all-start.4 = ((f32[8,16,256]{2,1,0:T(8,128)}), f32[8,16,256]{2,1,0:T(8,128)S(1)}, u32[]{:S(2)}, u32[]{:S(2)}) async-start(f32[8,16,256]{2,1,0:T(8,128)} %copy.34), calls=%async_computation.4 | async-start | bytes 262144 | tf_op jit(solution)/shard_map/all_to_all | solution.py:49
  100.2 3.4 %all-to-all-done.4 = f32[8,16,256]{2,1,0:T(8,128)S(1)} async-done(((f32[8,16,256]{2,1,0:T(8,128)}), f32[8,16,256]{2,1,0:T(8,128)S(1)}, u32[]{:S(2)}, u32[]{:S(2)}) %all-to-all-start.4) | async-done | bytes 131104 | tf_op jit(solution)/shard_map/all_to_all | solution.py:49
  106.1 8.6 %all-reduce.10 = (f32[4]{0:T(128)S(1)}, f32[4]{0:T(128)S(1)}) all-reduce(f32[4]{0:T(128)S(1)} %dynamic-update-slice, f32[4]{0:T(128)S(1)} %dynamic-update-slice.4), channel_id=1, replica_groups=mesh['fs_0'=4,'fs_1'=4,'tp_0'=4,'tp_1'=2] {'fs_0'}, use_global_device_ids=true, to_apply=%add | all-reduce | flops 8 | bytes 64
  115.9 1.4 dynamic-update-slice.1
  117.3 1.4 dynamic-update-slice.5
  119.3 8.8 %all-reduce.9 = (f32[4]{0:T(128)S(1)}, f32[4]{0:T(128)S(1)}) all-reduce(f32[4]{0:T(128)S(1)} %dynamic-update-slice.1, f32[4]{0:T(128)S(1)} %dynamic-update-slice.5), channel_id=1, replica_groups=mesh['fs_0'=4,'fs_1'=4,'tp_0'=4,'tp_1'=2] {'fs_1'}, use_global_device_ids=true, to_apply=%add.1 | all-reduce | flops 8 | bytes 64
  130.7 1.4 dynamic-update-slice.6
  132.7 8.9 %all-reduce.8 = (f32[4]{0:T(128)S(1)}, f32[4]{0:T(128)S(1)}) all-reduce(f32[4]{0:T(128)S(1)} %dynamic-update-slice.2, f32[4]{0:T(128)S(1)} %dynamic-update-slice.6), channel_id=1, replica_groups=mesh['fs_0'=4,'fs_1'=4,'tp_0'=4,'tp_1'=2] {'tp_0'}, use_global_device_ids=true, to_apply=%add.2 | all-reduce | flops 8 | bytes 64
  144.1 1.4 dynamic-update-slice.7
  145.6 2.5 %all-reduce.11 = (f32[2]{0:T(128)S(1)}, f32[2]{0:T(128)S(1)}) all-reduce(f32[2]{0:T(128)S(1)} %dynamic-update-slice.3, f32[2]{0:T(128)S(1)} %dynamic-update-slice.7), channel_id=1, replica_groups=mesh['fs_0'=4,'fs_1'=4,'tp_0'=4,'tp_1'=2] {'tp_1'}, use_global_device_ids=true, to_apply=%add.3 | all-reduce | flops 4 | bytes 32
  151.9 22.0 %all_gather.73 = f32[256,384]{1,0:T(8,128)S(1)} all-gather(f32[16,384]{1,0:T(8,128)S(1)} %pad_maximum_fusion.2), channel_id=1, replica_groups=mesh['fs_0'=4,'fs_1'=4,'tp_0'=4,'tp_1'=2] {'fs_0','fs_1'}, dimensions={0}, use_global_device_ids=true | all-gather | bytes 417792 | tf_op jit(solution)/shard_map/all_gather | solution.py:65
  178.0 37.2 %all-gather.3.cloned.1.call-done = bf16[524288]{0:T(1024)(128)(2,1)} async-done(((bf16[32768]{0:T(1024)(128)(2,1)}), bf16[524288]{0:T(1024)(128)(2,1)}) %all-gather.3.cloned.1.call-update) | async-done | bytes 1048592 | tf_op jit(solution)/shard_map/all_gather | solution.py:70
  215.3 1.5 reshape.49
  (89 shorter events, 26.7 us)
Async XLA Ops:
  29.4 19.9 %all-to-all-start = ((bf16[16,128,256]{2,1,0:T(8,128)(2,1)}), bf16[16,128,256]{2,1,0:T(8,128)(2,1)S(1)}, u32[]{:S(2)}, u32[]{:S(2)}) async-start(bf16[16,128,256]{2,1,0:T(8,128)(2,1)} %broadcast_in_dim.6), calls=%async_computation | async-start | bytes 2097152 | tf_op jit(solution)/shard_map/all_to_all | solution.py:22
  33.1 9.5 %slice-start = ((s8[8388608]{0:T(1024)(128)(4,1)}), s8[4194304]{0:T(1024)(128)(4,1)S(1)}, s32[]{:S(2)}) async-start(s8[8388608]{0:T(1024)(128)(4,1)} %bitcast.49), calls=%async_computation.6 | async-start | bytes 8388608
  36.7 5.9 %slice-start.1 = ((s8[8388608]{0:T(1024)(128)(4,1)}), s8[4194304]{0:T(1024)(128)(4,1)S(1)}, s32[]{:S(2)}) async-start(s8[8388608]{0:T(1024)(128)(4,1)} %bitcast.49), calls=%async_computation.7 | async-start | bytes 8388608
  49.4 6.0 %copy-start.8 = (bf16[2048,1024]{1,0:T(8,128)(2,1)S(1)}, bf16[2048,1024]{1,0:T(8,128)(2,1)}, u32[]{:S(2)}) copy-start(bf16[2048,1024]{1,0:T(8,128)(2,1)} %param.13) | copy-start | bytes 12582916
  83.2 14.4 %copy-start.12 = (u32[128]{0:T(128)S(1)}, u32[128]{0:T(128)}, u32[]{:S(2)}) copy-start(u32[128]{0:T(128)} %constant.8) | copy-start | bytes 1540
  83.2 22.3 %copy-start.11 = (u32[128]{0:T(128)S(1)}, u32[128]{0:T(128)}, u32[]{:S(2)}) copy-start(u32[128]{0:T(128)} %constant.37) | copy-start | bytes 1540
  83.2 35.5 %copy-start.10 = (u32[128]{0:T(128)S(1)}, u32[128]{0:T(128)}, u32[]{:S(2)}) copy-start(u32[128]{0:T(128)} %constant.42) | copy-start | bytes 1540
  83.2 48.9 %copy-start.9 = (u32[128]{0:T(128)S(1)}, u32[128]{0:T(128)}, u32[]{:S(2)}) copy-start(u32[128]{0:T(128)} %constant.47) | copy-start | bytes 1540
  83.2 62.3 %copy-start.3 = (f32[128,128]{1,0:T(8,128)S(1)}, f32[128,128]{1,0:T(8,128)}, u32[]{:S(2)}) copy-start(f32[128,128]{1,0:T(8,128)} %param.18) | copy-start | bytes 196612
  83.2 67.4 %copy-start.4 = (f32[16,256]{1,0:T(8,128)S(1)}, f32[16,256]{1,0:T(8,128)}, u32[]{:S(2)}) copy-start(f32[16,256]{1,0:T(8,128)} %param.23) | copy-start | bytes 49156
  83.2 67.4 %copy-start.5 = (f32[16,256]{1,0:T(8,128)S(1)}, f32[16,256]{1,0:T(8,128)}, u32[]{:S(2)}) copy-start(f32[16,256]{1,0:T(8,128)} %param.22) | copy-start | bytes 49156
  83.3 68.1 %copy-start.6 = (f32[16,128]{1,0:T(8,128)S(1)}, f32[16,128]{1,0:T(8,128)}, u32[]{:S(2)}) copy-start(f32[16,128]{1,0:T(8,128)} %param.21) | copy-start | bytes 24580
  83.3 68.1 %copy-start.7 = (f32[16,128]{1,0:T(8,128)S(1)}, f32[16,128]{1,0:T(8,128)}, u32[]{:S(2)}) copy-start(f32[16,128]{1,0:T(8,128)} %param.20) | copy-start | bytes 24580
  83.3 90.6 %copy-start.1 = (bf16[64,256]{1,0:T(8,128)(2,1)S(1)}, bf16[64,256]{1,0:T(8,128)(2,1)}, u32[]{:S(2)}) copy-start(bf16[64,256]{1,0:T(8,128)(2,1)} %param.17) | copy-start | bytes 98308
  83.3 90.8 %copy-start = (bf16[128,256]{1,0:T(8,128)(2,1)S(1)}, bf16[128,256]{1,0:T(8,128)(2,1)}, u32[]{:S(2)}) copy-start(bf16[128,256]{1,0:T(8,128)(2,1)} %param.16) | copy-start | bytes 196612
  83.5 90.9 %copy-start.2 = (f32[64,256]{1,0:T(8,128)S(1)}, f32[64,256]{1,0:T(8,128)}, u32[]{:S(2)}) copy-start(f32[64,256]{1,0:T(8,128)} %param.19) | copy-start | bytes 196612
  84.2 9.9 %all-to-all-start.3 = ((f32[8,16,128]{2,1,0:T(8,128)}), f32[8,16,128]{2,1,0:T(8,128)S(1)}, u32[]{:S(2)}, u32[]{:S(2)}) async-start(f32[8,16,128]{2,1,0:T(8,128)} %copy.33), calls=%async_computation.3 | async-start | bytes 131072 | tf_op jit(solution)/shard_map/all_to_all | solution.py:49
  94.1 9.4 %all-to-all-start.4 = ((f32[8,16,256]{2,1,0:T(8,128)}), f32[8,16,256]{2,1,0:T(8,128)S(1)}, u32[]{:S(2)}, u32[]{:S(2)}) async-start(f32[8,16,256]{2,1,0:T(8,128)} %copy.34), calls=%async_computation.4 | async-start | bytes 262144 | tf_op jit(solution)/shard_map/all_to_all | solution.py:49
  97.5 117.8 %all-gather.3.cloned.1.call-start = ((), (), s32[]{:S(2)}) async-start(), calls=%async_computation.5 | async-start | bytes 1114112 | tf_op jit(solution)/shard_map/all_gather | solution.py:70
Sparse Core Ops, SparseCore 0:
  176.0 39.1 all-gather.2
